TPU v7x, 32 devices: a whole 2x2x4 slice. The times are simulated.
32 devices in a mesh: sp: 4 (over y, x), dp: 8 (over z, core).
Axes of the slice: x: 2, y: 2, z: 4, core: 2. Of those that a mesh axis runs over, the one named last changes fastest.
Arguments:
- tokens: bfloat16 [8, 1024, 2048], P('dp', 'sp'), may hold values from -200 to 200
- w_qdown: bfloat16 [2048, 512], P('dp'), may hold values from -0.125 to 0.125
- w_kvdown: bfloat16 [2048, 512], P('dp'), may hold values from -0.125 to 0.125
- w_rotary: bfloat16 [2048, 64], replicated, may hold values from -0.125 to 0.125
- q_gain: float32 [512], replicated, may hold values from 0.1 to 1.9
- kv_gain: float32 [512], replicated, may hold values from 0.1 to 1.9
- w_qup: bfloat16 [512, 3072], P('dp'), may hold values from -1 to 1
- w_kvup: bfloat16 [512, 4096], P('dp'), may hold values from -1 to 1
- w_out: bfloat16 [2048, 2048], P(None, 'dp'), may hold values from -0.125 to 0.125
- out_gain: float32 [2048], replicated, may hold values from 0.1 to 1.9
Outputs:
- mixed: bfloat16 [8, 1024, 2048], P('dp', 'sp')
All inputs are finite; a program needn't handle non-finite values.
Results may differ from a plain program's by a relative error of at most 0.01.
The roundings to bfloat16 on the way count: a program that leaves them out, or rounds other values in their place, can miss the bound.
Values may be sent and summed in bfloat16 or wider, within the bound.
A program may use at most 128 MiB of HBM per device.

v0:
```python
import math
import jax
import jax.numpy as jnp
from jax import lax
from jax.sharding import PartitionSpec as P

HEADS = 16
NOPE = 128
ROPE = 64
VDIM = 128
EPSILON = 1e-06
THETA = 10000.0


def norm_rows(values, gain):
    scale = lax.rsqrt(jnp.mean(values * values, axis=-1, keepdims=True) + EPSILON)
    return values * scale * gain


def rotate(values, cosine, sine):
    half = values.shape[-1] // 2
    first = values[..., :half]
    second = values[..., half:]
    return jnp.concatenate(
        [first * cosine - second * sine, second * cosine + first * sine], axis=-1
    )


def turn_tables(offset, count):
    positions = (offset + jnp.arange(count)).astype(jnp.float32)
    freqs = THETA ** (-jnp.arange(0, ROPE, 2).astype(jnp.float32) / ROPE)
    angles = positions[:, None] * freqs[None, :]
    return (jnp.cos(angles), jnp.sin(angles))


def make_queries(q_full, cosine, sine, heads_here):
    rows = q_full.shape[0]
    shaped = q_full.reshape(rows, heads_here, NOPE + ROPE)
    turned = rotate(shaped[..., NOPE:], cosine[:, None, :], sine[:, None, :])
    joined = jnp.concatenate([shaped[..., :NOPE], turned], axis=-1)
    return joined.reshape(rows, heads_here * (NOPE + ROPE)).astype(jnp.bfloat16)


def attend(query_heads, keyval_heads, key_rot, heads_here):
    length = query_heads.shape[0]
    block = math.gcd(length, 512)
    scaling = (NOPE + ROPE) ** (-0.5)
    queries = query_heads.reshape(length, heads_here, NOPE + ROPE)
    keyval = keyval_heads.reshape(length, heads_here, NOPE + VDIM)
    keys_all = keyval[..., :NOPE]
    values_all = keyval[..., NOPE:]
    outputs = []
    for begin in range(0, length, block):
        finish = begin + block
        query_block = queries[begin:finish]
        scores = jnp.einsum(
            "qhd,khd->hqk",
            query_block[..., :NOPE],
            keys_all[:finish],
            preferred_element_type=jnp.float32,
        )
        scores = scores + jnp.einsum(
            "qhd,kd->hqk",
            query_block[..., NOPE:],
            key_rot[:finish],
            preferred_element_type=jnp.float32,
        )
        scores = scores * scaling
        query_pos = begin + jnp.arange(block)
        key_pos = jnp.arange(finish)
        allowed = key_pos[None, :] <= query_pos[:, None]
        scores = jnp.where(allowed[None], scores, -jnp.inf)
        top = jnp.max(scores, axis=-1, keepdims=True)
        expo = jnp.exp(scores - top)
        weights = (expo / jnp.sum(expo, axis=-1, keepdims=True)).astype(jnp.bfloat16)
        attended = jnp.einsum(
            "hqk,khd->qhd", weights, values_all[:finish], preferred_element_type=jnp.float32
        )
        outputs.append(attended.astype(jnp.bfloat16))
    return jnp.concatenate(outputs, axis=0).reshape(length, heads_here * VDIM)


def body(tokens, w_qdown, w_kvdown, w_rotary, q_gain, kv_gain, w_qup, w_kvup, w_out, out_gain):
    own_rows = tokens[0]
    tok_count = own_rows.shape[0]
    sp_count = lax.axis_size("sp")
    sp_place = lax.axis_index("sp")
    length = tok_count * sp_count
    heads_here = HEADS // sp_count
    pieces = (
        lax.all_gather(w_qdown, "dp", axis=0, tiled=True),
        lax.all_gather(w_kvdown, "dp", axis=0, tiled=True),
    )
    q_lat = jnp.dot(own_rows, pieces[0], preferred_element_type=jnp.float32)
    kv_lat = jnp.dot(own_rows, pieces[1], preferred_element_type=jnp.float32)
    q_norm = norm_rows(q_lat, q_gain).astype(jnp.bfloat16)
    kv_norm = norm_rows(kv_lat, kv_gain).astype(jnp.bfloat16)
    own_cos, own_sin = turn_tables(sp_place * tok_count, tok_count)
    key_rot = rotate(
        jnp.dot(own_rows, w_rotary, preferred_element_type=jnp.float32), own_cos, own_sin
    ).astype(jnp.bfloat16)
    q_all, kv_all, rot_all = (
        lax.all_gather(q_norm, "sp", axis=0, tiled=True),
        lax.all_gather(kv_norm, "sp", axis=0, tiled=True),
        lax.all_gather(key_rot, "sp", axis=0, tiled=True),
    )
    q_width = heads_here * (NOPE + ROPE)
    kv_width = heads_here * (NOPE + VDIM)
    q_columns = lax.dynamic_slice_in_dim(w_qup, sp_place * q_width, q_width, 1)
    kv_columns = lax.dynamic_slice_in_dim(w_kvup, sp_place * kv_width, kv_width, 1)
    pieces = (
        lax.all_gather(q_columns, "dp", axis=0, tiled=True),
        lax.all_gather(kv_columns, "dp", axis=0, tiled=True),
    )
    q_full = jnp.dot(q_all, pieces[0], preferred_element_type=jnp.float32)
    kv_full = jnp.dot(kv_all, pieces[1], preferred_element_type=jnp.float32)
    all_cos, all_sin = turn_tables(0, length)
    query_heads = make_queries(q_full, all_cos, all_sin, heads_here)
    keyval_heads = kv_full.astype(jnp.bfloat16)
    attended = attend(query_heads, keyval_heads, rot_all, heads_here)
    merged = lax.all_to_all(attended, "sp", split_axis=0, concat_axis=1, tiled=True)
    proj = jnp.dot(
        merged, lax.all_gather(w_out, "dp", axis=1, tiled=True), preferred_element_type=jnp.float32
    )
    mixed = norm_rows(proj, out_gain).astype(jnp.bfloat16)
    return mixed[None]


def solution(mesh):
    in_specs = (
        P("dp", "sp", None),
        P("dp", None),
        P("dp", None),
        P(),
        P(),
        P(),
        P("dp", None),
        P("dp", None),
        P(None, "dp"),
        P(),
    )
    out_specs = P("dp", "sp", None)
    return jax.shard_map(body, mesh=mesh, in_specs=in_specs, out_specs=out_specs, check_vma=False)
```

profile of v0, /device:TPU:0, one launch (start us, length us, event | category | flops | bytes accessed | tf_op | source)
XLA Modules:
  0.0 248.7 jit_solution(12525613199316772031)
XLA Ops:
  8.1 32.8 %all-gather.13.cloned.1.call-done = bf16[2048,512]{1,0:T(8,128)(2,1)} async-done(((bf16[256,512]{1,0:T(8,128)(2,1)}), bf16[2048,512]{1,0:T(8,128)(2,1)}) %all-gather.13.cloned.1.call-update) | async-done | bytes 2097168 | tf_op jit(solution)/shard_map/all_gather | solution.py:91
  40.8 2.4 multiply_reduce_fusion.1
  44.2 1.6 constant_dynamic-slice_fusion.1
  45.8 25.2 %all-gather.7.cloned.1.call-done = bf16[2048,512]{1,0:T(8,128)(2,1)} async-done(((bf16[256,512]{1,0:T(8,128)(2,1)}), bf16[2048,512]{1,0:T(8,128)(2,1)}) %all-gather.7.cloned.1.call-update) | async-done | bytes 2097168 | tf_op jit(solution)/shard_map/all_gather | solution.py:92
  71.0 2.4 multiply_reduce_fusion.2
  75.5 10.3 %all_gather.30 = bf16[1024,64]{0,1:T(8,128)(2,1)S(1)} all-gather(bf16[256,64]{0,1:T(8,128)(2,1)S(1)} %pad_maximum_fusion.3), channel_id=1, replica_groups=mesh['sp'=4,'dp'=8] {'sp'}, dimensions={0}, use_global_device_ids=true | all-gather | bytes 163840 | tf_op jit(solution)/shard_map/all_gather | solution.py:105
  90.0 15.7 %all_gather.29 = bf16[512,768]{1,0:T(8,128)(2,1)S(1)} all-gather(bf16[64,768]{1,0:T(8,128)(2,1)S(1)} %constant_dynamic-slice_fusion), channel_id=1, replica_groups=mesh['sp'=4,'dp'=8] {'dp'}, dimensions={0}, use_global_device_ids=true | all-gather | bytes 884736 | tf_op jit(solution)/shard_map/all_gather | solution.py:112
  105.7 4.0 %fusion.45 = f32[1024,768]{0,1:T(8,128)} fusion(bf16[1024,512]{1,0:T(8,128)(2,1)} %all-gather.15.cloned.1.call-done, bf16[512,768]{1,0:T(8,128)(2,1)S(1)} %all_gather.29), kind=kOutput, calls=%fused_computation.80 | convolution fusion | flops 805306368 | bytes 4980736 | tf_op jit(solution)/shard_map/dot_general | solution.py:115
  109.7 3.3 %copy.16 = bf16[1024,4,192]{2,0,1:T(8,128)(2,1)S(1)} copy(f32[1024,4,192]{0,2,1:T(8,128)} %bitcast.55) | data formatting | bytes 4718592 | tf_op jit(solution)/shard_map/reshape | solution.py:38
  112.9 2.1 subtract_convert_fusion
  115.1 7.9 %all-gather.11.cloned.1.call-done = bf16[512,1024]{1,0:T(8,128)(2,1)} async-done(((bf16[64,1024]{1,0:T(8,128)(2,1)}), bf16[512,1024]{1,0:T(8,128)(2,1)}) %all-gather.11.cloned.1.call-update) | async-done | bytes 1048592 | tf_op jit(solution)/shard_map/all_gather | solution.py:113
  123.0 27.8 %all-gather.9.cloned.1.call-done = bf16[1024,512]{1,0:T(8,128)(2,1)} async-done(((bf16[256,512]{1,0:T(8,128)(2,1)}), bf16[1024,512]{1,0:T(8,128)(2,1)}) %all-gather.9.cloned.1.call-update) | async-done | bytes 1048592 | tf_op jit(solution)/shard_map/all_gather | solution.py:104
  150.8 2.8 %convolution_convert_fusion = bf16[1024,1024]{0,1:T(8,128)(2,1)S(1)} fusion(bf16[1024,512]{1,0:T(8,128)(2,1)} %all-gather.9.cloned.1.call-done, bf16[512,1024]{1,0:T(8,128)(2,1)} %all-gather.11.cloned.1.call-done), kind=kOutput, calls=%fused_computation.17 | convolution fusion | flops 1074790400 | bytes 4194304 | tf_op jit(solution)/shard_map/dot_general | solution.py:116
  156.1 2.0 copy-done.2
  158.8 6.5 %fusion.11 = bf16[512,4,128]{0,2,1:T(8,128)(2,1)} fusion(f32[4,512]{1,0:T(4,128)S(1)} %fusion.44, bf16[1024,4,256]{0,2,1:T(8,128)(2,1)} %bitcast.59, f32[4,512,512]{1,2,0:T(8,128)} %copy-done.2), kind=kOutput, calls=%fused_computation.21 | convolution fusion | flops 271845888 | bytes 9445376 | tf_op jit(solution)/shard_map/hqk,khd->qhd/dot_general | solution.py:76
  165.4 2.4 fusion.28
  167.7 1.8 fusion.3
  169.6 3.2 %copy-done.1 = f32[4,512,1024]{2,1,0:T(8,128)} copy-done((f32[4,512,1024]{2,1,0:T(8,128)}, f32[4,512,1024]{2,1,0:T(8,128)S(1)}, u32[]{:S(2)}) %copy-start.1) | copy-done | bytes 8388632
  172.8 2.0 fusion.43
  174.9 11.1 %fusion.10 = bf16[512,4,128]{0,2,1:T(8,128)(2,1)} fusion(f32[4,512]{1,0:T(4,128)S(1)} %fusion.43, bf16[1024,4,256]{0,2,1:T(8,128)(2,1)S(1)} %bitcast.61, f32[4,512,1024]{2,1,0:T(8,128)} %copy-done.1), kind=kOutput, calls=%fused_computation.20 | convolution fusion | flops 543427584 | bytes 18358272 | tf_op jit(solution)/shard_map/hqk,khd->qhd/dot_general | solution.py:76
  186.0 1.3 pad_maximum_fusion
  188.3 16.8 %all_to_all.19 = bf16[4,256,512]{1,2,0:T(8,128)(2,1)S(1)} all-to-all(bf16[4,256,512]{1,2,0:T(8,128)(2,1)S(1)} %copy.21), channel_id=1, replica_groups=mesh['sp'=4,'dp'=8] {'sp'}, dimensions={0} | all-to-all | bytes 2097152 | tf_op jit(solution)/shard_map/all_to_all | solution.py:121
  205.1 29.7 %all-gather.17.cloned.1.call-done = bf16[2048,2048]{1,0:T(8,128)(2,1)} async-done(((bf16[2048,256]{1,0:T(8,128)(2,1)}), bf16[2048,2048]{1,0:T(8,128)(2,1)}) %all-gather.17.cloned.1.call-update) | async-done | bytes 8388624 | tf_op jit(solution)/shard_map/all_gather | solution.py:123
  234.8 5.8 %multiply_reduce_fusion = (f32[256]{0:T(256)S(1)}, f32[256,2048]{1,0:T(8,128)S(1)}) fusion(bf16[256,2048]{0,1:T(8,128)(2,1)S(1)} %bitcast.57, bf16[2048,2048]{1,0:T(8,128)(2,1)} %all-gather.17.cloned.1.call-done), kind=kOutput, calls=%fused_computation.14 | convolution fusion | flops 2148531968 | bytes 11535360 | tf_op jit(solution)/shard_map/dot_general | solution.py:122
  (59 shorter events, 14.0 us)
Async XLA Ops:
  6.5 34.3 %copy-start = (bf16[1,256,2048]{2,1,0:T(8,128)(2,1)S(1)}, bf16[1,256,2048]{2,1,0:T(8,128)(2,1)}, u32[]{:S(2)}) copy-start(bf16[1,256,2048]{2,1,0:T(8,128)(2,1)} %param.10) | copy-start | bytes 3145732
  6.5 36.7 %copy-start.11 = (f32[512]{0:T(512)S(1)}, f32[512]{0:T(512)}, u32[]{:S(2)}) copy-start(f32[512]{0:T(512)} %param.14) | copy-start | bytes 6148
  6.5 34.3 %all-gather.13.cloned.1.call-start = ((), (), s32[]{:S(2)}) async-start(), calls=%async_computation.4 | async-start | bytes 2359296 | tf_op jit(solution)/shard_map/all_gather | solution.py:91
  7.3 63.8 %all-gather.7.cloned.1.call-start = ((), (), s32[]{:S(2)}) async-start(), calls=%async_computation.1 | async-start | bytes 2359296 | tf_op jit(solution)/shard_map/all_gather | solution.py:92
  8.0 65.4 %copy-start.12 = (f32[512]{0:T(512)S(1)}, f32[512]{0:T(512)}, u32[]{:S(2)}) copy-start(f32[512]{0:T(512)} %param.15) | copy-start | bytes 6148
  8.0 97.7 %all-gather.15.cloned.1.call-start = ((), (), s32[]{:S(2)}) async-start(), calls=%async_computation.5 | async-start | bytes 1310720 | tf_op jit(solution)/shard_map/all_gather | solution.py:103
  43.2 31.7 %copy-start.9 = (bf16[2048,64]{0,1:T(8,128)(2,1)S(1)}, bf16[2048,64]{0,1:T(8,128)(2,1)}, u32[]{:S(2)}) copy-start(bf16[2048,64]{0,1:T(8,128)(2,1)} %param.13) | copy-start | bytes 786436
  44.1 78.9 %all-gather.11.cloned.1.call-start = ((), (), s32[]{:S(2)}) async-start(), calls=%async_computation.3 | async-start | bytes 1179648 | tf_op jit(solution)/shard_map/all_gather | solution.py:113
  45.8 105.0 %all-gather.9.cloned.1.call-start = ((), (), s32[]{:S(2)}) async-start(), calls=%async_computation.2 | async-start | bytes 1310720 | tf_op jit(solution)/shard_map/all_gather | solution.py:104
  74.3 160.5 %all-gather.17.cloned.1.call-start = ((), (), s32[]{:S(2)}) async-start(), calls=%async_computation.6 | async-start | bytes 9437184 | tf_op jit(solution)/shard_map/all_gather | solution.py:123
  153.7 1.3 copy-start.5
  153.7 1.3 copy-start.3
  153.7 1.4 copy-start.8
  156.1 2.0 copy-start.2
  165.4 2.4 copy-start.4
  165.4 2.4 copy-start.6
  169.6 3.2 %copy-start.1 = (f32[4,512,1024]{2,1,0:T(8,128)}, f32[4,512,1024]{2,1,0:T(8,128)S(1)}, u32[]{:S(2)}) copy-start(f32[4,512,1024]{2,1,0:T(8,128)S(1)} %fusion.3) | copy-start | bytes 25165828
  172.8 2.0 copy-start.7
  234.8 5.8 %copy-start.10 = (f32[2048]{0:T(1024)S(1)}, f32[2048]{0:T(1024)}, u32[]{:S(2)}) copy-start(f32[2048]{0:T(1024)} %param.19) | copy-start | bytes 24580
Sparse Core Ops, SparseCore 0:
  8.9 31.8 all-gather.12
  42.4 28.5 all-gather.6
  72.9 26.3 all-gather.14
  100.8 22.2 all-gather.10
  124.7 26.0 all-gather.8
  152.3 82.4 all-gather.16
where the time goes:
time: 249 us
  waiting for transfers between devices  125 us (50%)
  blocking collectives  42.8 us (17%)
  matrix products  41.4 us (17%)
  between operations  13.7 us (6%)
  other arithmetic  12.7 us (5%)
  local copies, waits for them, and re-layouts  12.5 us (5%)
    all_gather x1, waiting for transfers between devices, body(): lax.all_gather(w_qdown, 'dp', axis=0, tiled=True)  32.8 us
    all_gather x1, waiting for transfers between devices, body(): lax.all_gather(w_out, 'dp', axis=1, tiled=True)  29.7 us
    all_gather x1, waiting for transfers between devices, body(): lax.all_gather(kv_norm, 'sp', axis=0, tiled=True)  27.8 us
    all_gather x1, waiting for transfers between devices, body(): lax.all_gather(w_kvdown, 'dp', axis=0, tiled=True)  25.2 us
    dot_general x2, matrix products, attend(): jnp.einsum('hqk,khd->qhd', weights, values_all[:finish], preferred_elemen...  17.6 us
    all_to_all x1, blocking collectives, body(): lax.all_to_all(attended, 'sp', split_axis=0, concat_axis=1, tiled=True)  16.8 us
    all_gather x1, blocking collectives, body(): lax.all_gather(q_columns, 'dp', axis=0, tiled=True)  15.7 us
    all_gather x1, blocking collectives, body(): lax.all_gather(key_rot, 'sp', axis=0, tiled=True)  10.3 us
  transfers between devices with their start and end apart: 6, of which 5 were waited for; matrix products, arithmetic and copies ran while one was open for 21% of the time, Pallas kernels for 0%

commit v1 on v0

--- a/solution.py
+++ b/solution.py
@@ -10,6 +10,23 @@
 VDIM = 128
 EPSILON = 1e-06
 THETA = 10000.0
+
+
+def joined_along(blocks, dim):
+    blocks = jnp.moveaxis(blocks, 0, dim)
+    dims = blocks.shape
+    return blocks.reshape(*dims[:dim], dims[dim] * dims[dim + 1], *dims[dim + 2 :])
+
+
+def collect(value, axis, dim):
+    length = lax.axis_size(axis)
+    upward = [(i, (i + 1) % length) for i in range(length)]
+    blocks = [value]
+    while len(blocks) < length:
+        blocks.append(lax.ppermute(blocks[-1], axis, upward))
+    index = lax.axis_index(axis)
+    blocks = jnp.stack(blocks)[(index - jnp.arange(length)) % length]
+    return joined_along(blocks, dim)
 
 
 def norm_rows(values, gain):
@@ -101,7 +118,7 @@
     ).astype(jnp.bfloat16)
     q_all, kv_all, rot_all = (
         lax.all_gather(q_norm, "sp", axis=0, tiled=True),
-        lax.all_gather(kv_norm, "sp", axis=0, tiled=True),
+        collect(kv_norm, "sp", 0),
         lax.all_gather(key_rot, "sp", axis=0, tiled=True),
     )
     q_width = heads_here * (NOPE + ROPE)

time: 249 us -> 225 us (0.904)
  waiting for transfers between devices: 125 us -> 95.6 us
  blocking collectives: 42.8 us -> 45.9 us
    all_gather x1 -> x0, waiting for transfers between devices: 27.8 us -> none  [body(): lax.all_gather(kv_norm, 'sp', axis=0, tiled=True)]
    all_gather x1, waiting for transfers between devices: 25.2 us -> 9.78 us  [body(): lax.all_gather(w_kvdown, 'dp', axis=0, tiled=True)]
    all_gather x1, waiting for transfers between devices: 0.01 us -> 14.7 us  [body(): lax.all_gather(q_norm, 'sp', axis=0, tiled=True)]
    ppermute x0 -> x3, waiting for transfers between devices: none -> 13.4 us  [collect(): blocks.append(lax.ppermute(blocks[-1], axis, upward))]
    all_gather x1, waiting for transfers between devices: 7.94 us -> 0.01 us  [body(): lax.all_gather(kv_columns, 'dp', axis=0, tiled=True)]
    all_gather x1, waiting for transfers between devices: 29.7 us -> 24.6 us  [body(): lax.all_gather(w_out, 'dp', axis=1, tiled=True)]
    all_gather x1, blocking collectives: 15.7 us -> 18.9 us  [body(): lax.all_gather(q_columns, 'dp', axis=0, tiled=True)]
    unnamed x26 -> x24, local copies, waits for them, and re-layouts: 5.87 us -> 5.23 us
  transfers between devices with their start and end apart: 6 -> 8, of which waited for: 5 -> 6; matrix products, arithmetic and copies ran while one was open for 21% -> 24% of each run, Pallas kernels for 0% -> 0%
where the time goes in v1:
time: 225 us
  waiting for transfers between devices  95.6 us (42%)
  blocking collectives  45.9 us (20%)
  matrix products  42.6 us (19%)
  local copies, waits for them, and re-layouts  13.5 us (6%)
  between operations  13.4 us (6%)
  other arithmetic  11.6 us (5%)
  starting transfers between devices  2.25 us (1%)
    all_gather x1, waiting for transfers between devices, body(): lax.all_gather(w_qdown, 'dp', axis=0, tiled=True)  31.1 us
    all_gather x1, waiting for transfers between devices, body(): lax.all_gather(w_out, 'dp', axis=1, tiled=True)  24.6 us
    all_gather x1, blocking collectives, body(): lax.all_gather(q_columns, 'dp', axis=0, tiled=True)  18.9 us
    all_to_all x1, blocking collectives, body(): lax.all_to_all(attended, 'sp', split_axis=0, concat_axis=1, tiled=True)  16.6 us
    dot_general x2, matrix products, attend(): jnp.einsum('hqk,khd->qhd', weights, values_all[:finish], preferred_elemen...  16.3 us
    all_gather x1, waiting for transfers between devices, body(): lax.all_gather(q_norm, 'sp', axis=0, tiled=True)  14.7 us
    ppermute x3, waiting for transfers between devices, collect(): blocks.append(lax.ppermute(blocks[-1], axis, upward))  13.4 us
    all_gather x1, blocking collectives, body(): lax.all_gather(key_rot, 'sp', axis=0, tiled=True)  10.4 us
  transfers between devices with their start and end apart: 8, of which 6 were waited for; matrix products, arithmetic and copies ran while one was open for 24% of the time, Pallas kernels for 0%

profile of v1, /device:TPU:0, one launch (start us, length us, event | category | flops | bytes accessed | tf_op | source)
XLA Modules:
  0.0 224.9 jit_solution(14636101389494083188)
XLA Ops:
  9.7 31.1 %all-gather.10.cloned.1.call-done = bf16[2048,512]{1,0:T(8,128)(2,1)} async-done(((bf16[256,512]{1,0:T(8,128)(2,1)}), bf16[2048,512]{1,0:T(8,128)(2,1)}) %all-gather.10.cloned.1.call-update) | async-done | bytes 2097168 | tf_op jit(solution)/shard_map/all_gather | solution.py:108
  40.8 2.4 %multiply_reduce_fusion.1 = (f32[256]{0:T(256)S(1)}, f32[256,512]{1,0:T(8,128)S(1)}) fusion(bf16[2048,512]{1,0:T(8,128)(2,1)} %all-gather.10.cloned.1.call-done, bf16[1,256,2048]{2,1,0:T(8,128)(2,1)S(1)} %copy-done), kind=kOutput, calls=%fused_computation.45 | convolution fusion | flops 537132800 | bytes 3671040 | tf_op jit(solution)/shard_map/dot_general | solution.py:111
  47.1 18.9 %all_gather.25 = bf16[512,768]{1,0:T(8,128)(2,1)S(1)} all-gather(bf16[64,768]{1,0:T(8,128)(2,1)S(1)} %constant_dynamic-slice_fusion), channel_id=1, replica_groups=mesh['sp'=4,'dp'=8] {'dp'}, dimensions={0}, use_global_device_ids=true | all-gather | bytes 884736 | tf_op jit(solution)/shard_map/all_gather | solution.py:129
  66.1 9.8 %all-gather.6.cloned.1.call-done = bf16[2048,512]{1,0:T(8,128)(2,1)} async-done(((bf16[256,512]{1,0:T(8,128)(2,1)}), bf16[2048,512]{1,0:T(8,128)(2,1)}) %all-gather.6.cloned.1.call-update) | async-done | bytes 2097168 | tf_op jit(solution)/shard_map/all_gather | solution.py:109
  75.8 2.4 %multiply_reduce_fusion.2 = (f32[256]{0:T(256)S(1)}, f32[256,512]{1,0:T(8,128)S(1)}) fusion(bf16[2048,512]{1,0:T(8,128)(2,1)} %all-gather.6.cloned.1.call-done, bf16[1,256,2048]{2,1,0:T(8,128)(2,1)S(1)} %copy-done), kind=kOutput, calls=%fused_computation.47 | convolution fusion | flops 537132800 | bytes 3671040 | tf_op jit(solution)/shard_map/dot_general | solution.py:112
  81.1 6.6 %collective-permute-done = bf16[256,512]{1,0:T(8,128)(2,1)S(1)} collective-permute-done((bf16[256,512]{1,0:T(8,128)(2,1)S(1)}, bf16[256,512]{1,0:T(8,128)(2,1)S(1)}, u32[]{:S(2)}, u32[]{:S(2)}) %collective-permute-start) | collective-permute-done | bytes 262176 | tf_op jit(solution)/shard_map/ppermute | solution.py:26
  89.5 6.7 %collective-permute-done.1 = bf16[256,512]{1,0:T(8,128)(2,1)S(1)} collective-permute-done((bf16[256,512]{1,0:T(8,128)(2,1)S(1)}, bf16[256,512]{1,0:T(8,128)(2,1)S(1)}, u32[]{:S(2)}, u32[]{:S(2)}) %collective-permute-start.1) | collective-permute-done | bytes 262176 | tf_op jit(solution)/shard_map/ppermute | solution.py:26
  96.2 10.4 %all_gather.26 = bf16[1024,64]{0,1:T(8,128)(2,1)S(1)} all-gather(bf16[256,64]{0,1:T(8,128)(2,1)S(1)} %pad_maximum_fusion.4), channel_id=1, replica_groups=mesh['sp'=4,'dp'=8] {'sp'}, dimensions={0}, use_global_device_ids=true | all-gather | bytes 163840 | tf_op jit(solution)/shard_map/all_gather | solution.py:122
  106.9 1.6 gather_fusion
  108.5 4.2 %convolution_convert_fusion = bf16[1024,1024]{0,1:T(8,128)(2,1)} fusion(bf16[1024,512]{1,0:T(8,128)(2,1)} %bitcast.70, bf16[512,1024]{1,0:T(8,128)(2,1)} %all-gather.8.cloned.1.call-done), kind=kOutput, calls=%fused_computation.18 | convolution fusion | flops 1074790400 | bytes 4194304 | tf_op jit(solution)/shard_map/dot_general | solution.py:133
  112.7 14.7 %all-gather.12.cloned.1.call-done = bf16[1024,512]{1,0:T(8,128)(2,1)} async-done(((bf16[256,512]{1,0:T(8,128)(2,1)}), bf16[1024,512]{1,0:T(8,128)(2,1)}) %all-gather.12.cloned.1.call-update) | async-done | bytes 1048592 | tf_op jit(solution)/shard_map/all_gather | solution.py:120
  127.4 4.0 %fusion.47 = f32[1024,768]{0,1:T(8,128)} fusion(bf16[1024,512]{1,0:T(8,128)(2,1)} %all-gather.12.cloned.1.call-done, bf16[512,768]{1,0:T(8,128)(2,1)S(1)} %all_gather.25), kind=kOutput, calls=%fused_computation.89 | convolution fusion | flops 805306368 | bytes 4980736 | tf_op jit(solution)/shard_map/dot_general | solution.py:132
  131.4 3.1 %copy.16 = bf16[1024,4,192]{2,0,1:T(8,128)(2,1)S(1)} copy(f32[1024,4,192]{0,2,1:T(8,128)} %bitcast.63) | data formatting | bytes 4718592 | tf_op jit(solution)/shard_map/reshape | solution.py:55
  136.1 2.0 fusion.22
  139.0 2.0 copy-done.2
  141.8 5.7 %fusion.11 = bf16[512,4,128]{0,2,1:T(8,128)(2,1)} fusion(f32[4,512]{1,0:T(4,128)S(1)} %fusion.46, bf16[1024,4,256]{0,2,1:T(8,128)(2,1)} %bitcast.67, f32[4,512,512]{1,2,0:T(8,128)} %copy-done.2), kind=kOutput, calls=%fused_computation.22 | convolution fusion | flops 271845888 | bytes 9445376 | tf_op jit(solution)/shard_map/hqk,khd->qhd/dot_general | solution.py:93
  147.5 2.3 %fusion.28 = f32[1024,512,4]{0,1,2:T(8,128)S(1)} fusion(bf16[1024,4,32]{0,2,1:T(8,128)(2,1)} %copy-done.3, bf16[1024,4,32]{0,2,1:T(8,128)(2,1)S(1)} %get-tuple-element.5, bf16[1024,64]{0,1:T(8,128)(2,1)S(1)} %all_gather.26), kind=kOutput, calls=%fused_computation.50 | convolution fusion | flops 268959744 | bytes 9043968 | tf_op jit(solution)/shard_map/qhd,kd->hqk/dot_general | solution.py:79
  149.8 1.8 fusion.3
  151.7 3.2 %copy-done.1 = f32[4,512,1024]{2,1,0:T(8,128)} copy-done((f32[4,512,1024]{2,1,0:T(8,128)}, f32[4,512,1024]{2,1,0:T(8,128)S(1)}, u32[]{:S(2)}) %copy-start.1) | copy-done | bytes 8388632
  154.9 2.0 fusion.45
  157.0 10.6 %fusion.10 = bf16[512,4,128]{0,2,1:T(8,128)(2,1)} fusion(f32[4,512]{1,0:T(4,128)S(1)} %fusion.45, bf16[1024,4,256]{0,2,1:T(8,128)(2,1)S(1)} %bitcast.69, f32[4,512,1024]{2,1,0:T(8,128)} %copy-done.1), kind=kOutput, calls=%fused_computation.21 | convolution fusion | flops 543427584 | bytes 18358272 | tf_op jit(solution)/shard_map/hqk,khd->qhd/dot_general | solution.py:93
  170.1 16.6 %all_to_all.19 = bf16[4,256,512]{1,2,0:T(8,128)(2,1)S(1)} all-to-all(bf16[4,256,512]{1,2,0:T(8,128)(2,1)S(1)} %copy.21), channel_id=1, replica_groups=mesh['sp'=4,'dp'=8] {'sp'}, dimensions={0} | all-to-all | bytes 2097152 | tf_op jit(solution)/shard_map/all_to_all | solution.py:138
  186.7 24.6 %all-gather.14.cloned.1.call-done = bf16[2048,2048]{1,0:T(8,128)(2,1)} async-done(((bf16[2048,256]{1,0:T(8,128)(2,1)}), bf16[2048,2048]{1,0:T(8,128)(2,1)}) %all-gather.14.cloned.1.call-update) | async-done | bytes 8388624 | tf_op jit(solution)/shard_map/all_gather | solution.py:140
  211.3 5.8 %multiply_reduce_fusion = (f32[256]{0:T(256)S(1)}, f32[256,2048]{1,0:T(8,128)S(1)}) fusion(bf16[256,2048]{0,1:T(8,128)(2,1)S(1)} %bitcast.65, bf16[2048,2048]{1,0:T(8,128)(2,1)} %all-gather.14.cloned.1.call-done), kind=kOutput, calls=%fused_computation.15 | convolution fusion | flops 2148531968 | bytes 11535360 | tf_op jit(solution)/shard_map/dot_general | solution.py:139
  (65 shorter events, 18.9 us)
Async XLA Ops:
  6.5 34.3 %copy-start = (bf16[1,256,2048]{2,1,0:T(8,128)(2,1)S(1)}, bf16[1,256,2048]{2,1,0:T(8,128)(2,1)}, u32[]{:S(2)}) copy-start(bf16[1,256,2048]{2,1,0:T(8,128)(2,1)} %param.10) | copy-start | bytes 3145732
  6.5 36.7 %copy-start.11 = (f32[512]{0:T(512)S(1)}, f32[512]{0:T(512)}, u32[]{:S(2)}) copy-start(f32[512]{0:T(512)} %param.14) | copy-start | bytes 6148
  6.5 38.2 %copy-start.8 = (bf16[2048,64]{0,1:T(8,128)(2,1)S(1)}, bf16[2048,64]{0,1:T(8,128)(2,1)}, u32[]{:S(2)}) copy-start(bf16[2048,64]{0,1:T(8,128)(2,1)} %param.13) | copy-start | bytes 786436
  6.5 34.3 %all-gather.10.cloned.1.call-start = ((), (), s32[]{:S(2)}) async-start(), calls=%async_computation.3 | async-start | bytes 2359296 | tf_op jit(solution)/shard_map/all_gather | solution.py:108
  7.3 68.6 %all-gather.6.cloned.1.call-start = ((), (), s32[]{:S(2)}) async-start(), calls=%async_computation.1 | async-start | bytes 2359296 | tf_op jit(solution)/shard_map/all_gather | solution.py:109
  8.0 100.5 %all-gather.8.cloned.1.call-start = ((), (), s32[]{:S(2)}) async-start(), calls=%async_computation.2 | async-start | bytes 1179648 | tf_op jit(solution)/shard_map/all_gather | solution.py:130
  9.7 117.7 %all-gather.12.cloned.1.call-start = ((), (), s32[]{:S(2)}) async-start(), calls=%async_computation.4 | async-start | bytes 1310720 | tf_op jit(solution)/shard_map/all_gather | solution.py:120
  44.1 34.2 %copy-start.10 = (f32[512]{0:T(512)S(1)}, f32[512]{0:T(512)}, u32[]{:S(2)}) copy-start(f32[512]{0:T(512)} %param.15) | copy-start | bytes 6148
  44.1 167.2 %all-gather.14.cloned.1.call-start = ((), (), s32[]{:S(2)}) async-start(), calls=%async_computation.5 | async-start | bytes 9437184 | tf_op jit(solution)/shard_map/all_gather | solution.py:140
  78.4 9.4 %collective-permute-start = (bf16[256,512]{1,0:T(8,128)(2,1)S(1)}, bf16[256,512]{1,0:T(8,128)(2,1)S(1)}, u32[]{:S(2)}, u32[]{:S(2)}) collective-permute-start(bf16[256,512]{1,0:T(8,128)(2,1)S(1)} %multiply_convert_fusion.2), channel_id=1, source_target_pairs={{0,8},{8,16},{16,24},{24,0},{1,9},{9,17},{17,25},{25,1},{2,10},{10... | collective-permute-start | bytes 786440 | tf_op jit(solution)/shard_map/ppermute | solution.py:26
  87.7 8.5 %collective-permute-start.1 = (bf16[256,512]{1,0:T(8,128)(2,1)S(1)}, bf16[256,512]{1,0:T(8,128)(2,1)S(1)}, u32[]{:S(2)}, u32[]{:S(2)}) collective-permute-start(bf16[256,512]{1,0:T(8,128)(2,1)S(1)} %collective-permute-done), channel_id=1, source_target_pairs={{0,8},{8,16},{16,24},{24,0},{1,9},{9,17},{17,25},{25,1},{2,10},{10... | collective-permute-start | bytes 786440 | tf_op jit(solution)/shard_map/ppermute | solution.py:26
  96.2 10.5 %collective-permute-start.2 = (bf16[256,512]{1,0:T(8,128)(2,1)S(1)}, bf16[256,512]{1,0:T(8,128)(2,1)S(1)}, u32[]{:S(2)}, u32[]{:S(2)}) collective-permute-start(bf16[256,512]{1,0:T(8,128)(2,1)S(1)} %collective-permute-done.1), channel_id=1, source_target_pairs={{0,8},{8,16},{16,24},{24,0},{1,9},{9,17},{17,25},{25,1},{2,10},{10... | collective-permute-start | bytes 786440 | tf_op jit(solution)/shard_map/ppermute | solution.py:26
  134.4 3.6 %copy-start.7 = (pred[512,512]{0,1:T(8,128)(4,1)S(1)}, pred[512,512]{0,1:T(8,128)(4,1)}, u32[]{:S(2)}) copy-start(pred[512,512]{0,1:T(8,128)(4,1)} %iota_compare_fusion.1) | copy-start | bytes 786436
  136.0 2.0 copy-start.3
  139.0 2.0 copy-start.2
  147.5 2.4 %copy-start.4 = (pred[512,1024]{1,0:T(8,128)(4,1)S(1)}, pred[512,1024]{1,0:T(8,128)(4,1)}, u32[]{:S(2)}) copy-start(pred[512,1024]{1,0:T(8,128)(4,1)} %iota_compare_fusion) | copy-start | bytes 1572868
  147.5 2.4 %copy-start.5 = (bf16[1024,1024]{0,1:T(8,128)(2,1)S(1)}, bf16[1024,1024]{0,1:T(8,128)(2,1)}, u32[]{:S(2)}) copy-start(bf16[1024,1024]{0,1:T(8,128)(2,1)} %convolution_convert_fusion) | copy-start | bytes 6291460
  151.7 3.2 %copy-start.1 = (f32[4,512,1024]{2,1,0:T(8,128)}, f32[4,512,1024]{2,1,0:T(8,128)S(1)}, u32[]{:S(2)}) copy-start(f32[4,512,1024]{2,1,0:T(8,128)S(1)} %fusion.3) | copy-start | bytes 25165828
  154.9 2.0 copy-start.6
  211.3 5.8 %copy-start.9 = (f32[2048]{0:T(1024)S(1)}, f32[2048]{0:T(1024)}, u32[]{:S(2)}) copy-start(f32[2048]{0:T(1024)} %param.19) | copy-start | bytes 24580
Sparse Core Ops, SparseCore 0:
  8.9 31.8 all-gather.9
  42.4 33.3 all-gather.5
  77.4 22.0 all-gather.7
  101.2 26.0 all-gather.11
  128.8 82.4 all-gather.13
